TPU v7x, 256 devices: a 8x8x2 block of a 8x8x16 slice. The times are simulated.
256 devices in a mesh: grp: 2 (over z), st: 16 (over y, core), tp: 8 (over x).
Axes of the slice: x: 8, y: 8, z: 2, core: 2. Of those that a mesh axis runs over, the one named last changes fastest.
The devices are a block of a 8x8x16 slice.
Arguments:
- tokens: bfloat16 [32768, 2048], P(('grp', 'st')), parts along dimension 0, may hold values from -6 to 6
- w_query: bfloat16 [2048, 512], P(None, 'tp'), may hold values from -0.125 to 0.125
- w_key: bfloat16 [2048, 512], P(None, 'tp'), may hold values from -0.125 to 0.125
- w_value: bfloat16 [2048, 1024], P(None, 'tp'), may hold values from -0.125 to 0.125
- w_decay: bfloat16 [2048, 512], P(None, 'tp'), may hold values from -0.125 to 0.125
- decay_rate: float32 [512], P('tp'), may hold values from 0.0002 to 0.04
- block_scale: float32 [256], P(('grp', 'st')), parts along dimension 0, may hold values from 0.5 to 2
- w_rquery: bfloat16 [2048, 1024], P(None, 'tp'), may hold values from -0.125 to 0.125
- w_gate: bfloat16 [2048, 1024], P(None, 'tp'), may hold values from -0.125 to 0.125
- w_rkey: bfloat16 [2048, 1024], P(None, 'tp'), may hold values from -0.125 to 0.125
- w_rvalue: bfloat16 [2048, 1024], P(None, 'tp'), may hold values from -3 to 3
- query_gain: float32 [128], replicated, may hold values from 0.1 to 1.9
- key_gain: float32 [128], replicated, may hold values from 0.1 to 1.9
- out_gain: float32 [1024], P('tp'), may hold values from 0.1 to 1.9
- store: bfloat16 [384, 128, 2048], P(('grp', 'st')), parts along dimension 0, may hold values from -6 to 6
- passage_ids: int32 [256, 4], P(('grp', 'st')), parts along dimension 0, may hold values from 0 to 191, as said below
Outputs:
- output: bfloat16 [32768, 1024], P(('grp', 'st'), 'tp'), parts along dimension 0
There are 2 independent parts, one for each index of `grp`. A program takes and returns all parts, laid end to end along the dimension named above; an argument that names none is the same for every part. Nothing has to cross between parts.
Inputs may be any that keep to these rules, and one draw needn't show every extreme that they name: `passage_ids`: passage p is held by index p // 12 of st. The 32 reads of the blocks of one index of st name passages of exactly 16 indices of st, exactly 2 reads of each; among them are always the index before its own and the index half the axis away.
All inputs are finite; a program needn't handle non-finite values.
Results may differ from a plain program's by a relative error of at most 0.0044.
Values may be sent and summed in bfloat16 or wider, within the bound.
No kernel may reach another device: no remote copies, remote signals or barrier semaphores. Data moves between devices by JAX's collectives and lax.ppermute only.
A program may use at most 128 MiB of HBM per device.

v0:
```python
import jax
import jax.numpy as jnp
from jax import lax
from jax.sharding import PartitionSpec as P

HEADS = 8
DK = 64
DV = 128
BLK = 128
NPASS = 4


EPS = 1e-06
PRECISE = lax.Precision.HIGHEST


def sent_to_all(array, axis):
    copies = jnp.broadcast_to(array, (lax.axis_size(axis), *array.shape))
    return lax.all_to_all(copies, axis, split_axis=0, concat_axis=0, tiled=True)


def of_everyone(array, axis):
    everything = sent_to_all(array, axis)
    return jnp.sum(everything, axis=0)


def head_norm(values, gain_row):
    return values * lax.rsqrt(jnp.mean(values * values, axis=-1, keepdims=True) + EPS) * gain_row


def gla_blocks(gla_query, gla_key, gla_value, log_decay):
    head_dim = gla_query.shape[-1]
    block_len = gla_query.shape[1]
    cumulative = jnp.cumsum(log_decay, axis=1)
    query_dec = gla_query * head_dim ** (-0.5) * jnp.exp(cumulative)
    key_dec = gla_key * jnp.exp(-cumulative)
    causal_mask = jnp.arange(block_len)[:, None] >= jnp.arange(block_len)[None, :]
    scores = jnp.einsum("nihd,njhd->nhij", query_dec, key_dec, precision=PRECISE)
    scores = jnp.where(causal_mask, scores, 0.0)
    within = jnp.einsum("nhij,njhv->nihv", scores, gla_value, precision=PRECISE)
    block_total = cumulative[:, -1:]
    update = jnp.einsum(
        "njhd,njhv->nhdv", gla_key * jnp.exp(block_total - cumulative), gla_value, precision=PRECISE
    )
    carry_decay = jnp.exp(block_total[:, 0])

    def advance(carry_state, block_item):
        query_part, state_delta, factor = block_item
        result = jnp.einsum("ihd,hdv->ihv", query_part, carry_state, precision=PRECISE)
        return (factor[..., None] * carry_state + state_delta, result)

    start_state = jnp.zeros((gla_query.shape[2], head_dim, gla_value.shape[-1]), jnp.float32)
    _, carried = lax.scan(advance, start_state, (query_dec, update, carry_decay))
    return within + carried


def on_device(
    tokens,
    w_query,
    w_key,
    w_value,
    w_decay,
    decay_rate,
    block_scale,
    w_rquery,
    w_gate,
    w_rkey,
    w_rvalue,
    query_gain,
    key_gain,
    out_gain,
    store,
    passage_ids,
):
    length = tokens.shape[0]
    num_blocks = length // BLK
    local_heads = w_value.shape[1] // DV
    gla_q = jnp.dot(tokens, w_query, preferred_element_type=jnp.float32)
    gla_k = jnp.dot(tokens, w_key, preferred_element_type=jnp.float32)
    gla_v = jnp.dot(tokens, w_value, preferred_element_type=jnp.float32)
    decay_pre = jnp.dot(tokens, w_decay, preferred_element_type=jnp.float32)
    log_decay = (
        -2.0
        * decay_rate[None, :]
        * jax.nn.sigmoid(decay_pre)
        * jnp.repeat(block_scale, BLK)[:, None]
    )

    def shaped(values, width):
        return values.reshape(num_blocks, BLK, local_heads, width)

    gla_out = gla_blocks(
        shaped(gla_q, DK), shaped(gla_k, DK), shaped(gla_v, DV), shaped(log_decay, DK)
    )
    gla_out = gla_out.reshape(length, local_heads * DV)
    stores_here = store.shape[0]
    passage_rows = store.shape[1]
    width = store.shape[2]
    st_size = lax.axis_size("st")
    request_count = passage_ids.shape[0] * passage_ids.shape[1]
    owner_count = min(st_size, request_count // 2)
    most = request_count // owner_count
    flat_ids = passage_ids.reshape(-1)
    owner_index = flat_ids // stores_here
    local_row = flat_ids % stores_here
    request_index = jnp.arange(request_count, dtype=jnp.int32)
    earlier = (owner_index[:, None] == owner_index[None, :]) & (
        request_index[None, :] < request_index[:, None]
    )
    rank_index = jnp.sum(earlier.astype(jnp.int32), axis=1)
    slot_index = owner_index * most + rank_index
    placed = slot_index[:, None] == jnp.arange(st_size * most, dtype=jnp.int32)[None, :]
    wanted = jnp.sum(jnp.where(placed, local_row[:, None] + 1, 0), axis=0) - 1
    incoming = lax.all_to_all(
        wanted.reshape(st_size, most), "st", split_axis=0, concat_axis=0, tiled=True
    )
    held_rows = jnp.take(store, jnp.maximum(incoming.reshape(-1), 0), axis=0)
    flat_rows = held_rows.reshape(st_size * most * passage_rows, width)
    made_keys = jnp.dot(flat_rows, w_rkey, preferred_element_type=jnp.float32).astype(jnp.bfloat16)
    made_values = jnp.dot(flat_rows, w_rvalue, preferred_element_type=jnp.float32).astype(
        jnp.bfloat16
    )
    made_keys = made_keys.reshape(st_size * most, passage_rows, local_heads * DV)
    made_values = made_values.reshape(st_size * most, passage_rows, local_heads * DV)
    back_keys, back_values = (
        lax.all_to_all(made_keys, "st", split_axis=0, concat_axis=0, tiled=True),
        lax.all_to_all(made_values, "st", split_axis=0, concat_axis=0, tiled=True),
    )
    passage_keys = jnp.take(back_keys, slot_index, axis=0).reshape(
        request_count * passage_rows, local_heads * DV
    )
    passage_values = jnp.take(back_values, slot_index, axis=0).reshape(
        request_count * passage_rows, local_heads * DV
    )
    key_rows = NPASS * passage_rows
    key_normed = head_norm(
        passage_keys.astype(jnp.float32).reshape(num_blocks, key_rows, local_heads, DV), key_gain
    ).astype(jnp.bfloat16)
    value_rows = passage_values.reshape(num_blocks, key_rows, local_heads, DV)
    read_query = jnp.dot(tokens, w_rquery, preferred_element_type=jnp.float32).reshape(
        num_blocks, BLK, local_heads, DV
    )
    read_query = head_norm(read_query, query_gain).astype(jnp.bfloat16)
    scores = jnp.einsum(
        "nqhd,nkhd->nhqk", read_query, key_normed, preferred_element_type=jnp.float32
    ) * DV ** (-0.5)
    expd = jnp.exp(scores)
    read_weight = (expd / jnp.sum(expd, axis=-1, keepdims=True)).astype(jnp.bfloat16)
    retrieved = jnp.einsum(
        "nhqk,nkhd->nqhd", read_weight, value_rows, preferred_element_type=jnp.float32
    )
    retrieved = retrieved.reshape(length, local_heads * DV)
    gate_value = jax.nn.sigmoid(jnp.dot(tokens, w_gate, preferred_element_type=jnp.float32))
    combined = gla_out + gate_value * retrieved
    square_sum = of_everyone(jnp.sum(combined * combined, axis=1), "tp")
    scale_rows = lax.rsqrt(square_sum / (HEADS * DV) + EPS)
    return (combined * scale_rows[:, None] * out_gain[None, :]).astype(jnp.bfloat16)


def solution(mesh):
    return jax.shard_map(
        on_device,
        mesh=mesh,
        in_specs=(
            P(("grp", "st"), None),
            P(None, "tp"),
            P(None, "tp"),
            P(None, "tp"),
            P(None, "tp"),
            P("tp"),
            P(("grp", "st")),
            P(None, "tp"),
            P(None, "tp"),
            P(None, "tp"),
            P(None, "tp"),
            P(),
            P(),
            P("tp"),
            P(("grp", "st"), None, None),
            P(("grp", "st"), None),
        ),
        out_specs=P(("grp", "st"), "tp"),
        check_vma=False,
    )
```

profile of v0, /device:TPU:513, one launch (start us, length us, event | category | flops | bytes accessed | tf_op | source)
XLA Modules:
  0.0 176.0 jit_solution(7136868946790092421)
XLA Ops:
  3.0 23.7 %all-to-all-start = ((s32[16,1,2]{2,1,0:T(1,128)}), s32[16,1,2]{2,1,0:T(1,128)S(1)}, u32[]{:S(2)}, u32[]{:S(2)}) async-start(s32[16,1,2]{2,1,0:T(1,128)} %bitcast.12), calls=%async_computation | async-start | bytes 16384 | tf_op jit(solution)/shard_map/all_to_all | solution.py:114
  28.0 3.7 %fusion.21 = f32[8,8,8,128]{3,1,2,0:T(8,128)S(1)} fusion(bf16[1024,2048]{1,0:T(8,128)(2,1)} %param.20, bf16[2048,64]{0,1:T(8,128)(2,1)} %param.24, f32[1024]{0:T(1024)S(1)} %broadcast_bitcast_fusion.1, f32[64]{0:T(128)S(1)} %broadcast_multiply_fusion), kind=kOutput, calls=%fused_computation.41 | convolution fusion | flops 268763136 | bytes 4722944 | tf_op jit(solution)/shard_map/dot_general | solution.py:81
  32.1 23.3 %fusion.37 = f32[8,128,1,64]{3,0,1,2:T(8,128)S(1)} fusion(f32[8,128,1,64]{3,0,1,2:T(8,128)S(1)} %copy.122), kind=kOutput, calls=%fused_computation.95 | output fusion | flops 8323072 | bytes 524288 | tf_op jit(solution)/shard_map/jit(cumsum)/reduce_window_sum | solution.py:34
  55.6 3.6 %fusion.38 = f32[1024,128]{1,0:T(8,128)S(1)} fusion(bf16[1024,2048]{1,0:T(8,128)(2,1)} %param.20, bf16[2048,128]{1,0:T(8,128)(2,1)S(1)} %copy-done.6), kind=kOutput, calls=%fused_computation.96 | convolution fusion | flops 536870912 | bytes 5242880 | tf_op jit(solution)/shard_map/dot_general | solution.py:80
  59.2 1.4 convolution_multiply_fusion
  62.1 10.0 %gather_fusion = bf16[32,128,2048]{2,1,0:T(8,128)(2,1)} fusion(bf16[12,128,2048]{2,1,0:T(8,128)(2,1)} %param.34, s32[1024]{0:T(1024)S(1)} %pad_clamp_fusion.1), kind=kCustom, calls=%fused_computation.2 | custom fusion | bytes 33554560 | tf_op jit(solution)/shard_map/jit(_take)/gather | solution.py:117
  72.1 9.1 %bitcast_select_fusion = bf16[4096,2048]{1,0:T(8,128)(2,1)S(1)} fusion(bf16[32,128,2048]{2,1,0:T(8,128)(2,1)} %gather_fusion, pred[4096]{0:T(1024)(128)(4,1)S(1)} %broadcast_bitcast_fusion), kind=kLoop, calls=%fused_computation.14 | loop fusion | flops 8388608 | bytes 33558528 | tf_op jit(solution)/shard_map/jit(_take)/select_n | solution.py:117
  81.2 6.1 %convolution_convert_fusion = bf16[4096,128]{1,0:T(8,128)(2,1)} fusion(bf16[4096,2048]{1,0:T(8,128)(2,1)S(1)} %bitcast_select_fusion, bf16[2048,128]{1,0:T(8,128)(2,1)S(1)} %copy-done), kind=kOutput, calls=%fused_computation.15 | convolution fusion | flops 2148007936 | bytes 18350080 | tf_op jit(solution)/shard_map/dot_general | solution.py:119
  87.3 7.3 %all-to-all-start.2 = ((bf16[32,128,128]{2,1,0:T(8,128)(2,1)}), bf16[32,128,128]{2,1,0:T(8,128)(2,1)S(1)}, u32[]{:S(2)}, u32[]{:S(2)}) async-start(bf16[32,128,128]{2,1,0:T(8,128)(2,1)} %bitcast.150), calls=%async_computation.2 | async-start | bytes 2097152 | tf_op jit(solution)/shard_map/all_to_all | solution.py:126
  94.7 3.7 %convolution_bitcast_fusion.3 = f32[8,8,8,128]{3,2,1,0:T(8,128)S(1)} fusion(bf16[1024,2048]{1,0:T(8,128)(2,1)} %param.20, bf16[2048,64]{0,1:T(8,128)(2,1)S(1)} %copy-done.8), kind=kOutput, calls=%fused_computation.34 | convolution fusion | flops 268435456 | bytes 4718592 | tf_op jit(solution)/shard_map/dot_general | solution.py:79
  99.9 9.2 %convolution_convert_fusion.1 = bf16[4096,128]{1,0:T(8,128)(2,1)} fusion(bf16[4096,2048]{1,0:T(8,128)(2,1)} %copy-done.3, bf16[2048,128]{1,0:T(8,128)(2,1)S(1)} %copy-done.12), kind=kOutput, calls=%fused_computation.16 | convolution fusion | flops 2148007936 | bytes 18350080 | tf_op jit(solution)/shard_map/dot_general | solution.py:120
  109.1 13.6 %all-to-all-done.2 = bf16[32,128,128]{2,1,0:T(8,128)(2,1)S(1)} async-done(((bf16[32,128,128]{2,1,0:T(8,128)(2,1)}), bf16[32,128,128]{2,1,0:T(8,128)(2,1)S(1)}, u32[]{:S(2)}, u32[]{:S(2)}) %all-to-all-start.2) | async-done | bytes 1048608 | tf_op jit(solution)/shard_map/all_to_all | solution.py:126
  122.6 4.4 %all-to-all-start.1 = ((bf16[32,128,128]{2,1,0:T(8,128)(2,1)}), bf16[32,128,128]{2,1,0:T(8,128)(2,1)}, u32[]{:S(2)}, u32[]{:S(2)}) async-start(bf16[32,128,128]{2,1,0:T(8,128)(2,1)} %bitcast.149), calls=%async_computation.1 | async-start | bytes 2097152 | tf_op jit(solution)/shard_map/all_to_all | solution.py:127
  127.1 16.0 %while.13 = (s32[]{:T(128)}, f32[1,64,128]{2,1,0:T(8,128)S(1)}, f32[8,128,1,128]{3,1,2,0:T(8,128)}, f32[8,1,64]{2,1,0:T(1,128)S(1)}, f32[8,1,64,128]{3,2,1,0:T(8...) while((s32[]{:T(128)}, f32[1,64,128]{2,1,0:T(8,128)S(1)}, ...), condition=%wide.region_2.3_spmd.clone, body=%wide.region_1.2_spmd.clone.sunk | while | flops 12615683 | bytes 296300 | solution.py:53
  127.1 1.1 constant_dynamic-slice_fusion.3
  139.1 1.1 constant_dynamic-slice_fusion.3
  144.1 1.7 fusion.15
  146.0 3.6 %multiply_reduce_fusion.2 = (f32[1024]{0:T(1024)S(1)}, f32[1024,128]{1,0:T(8,128)S(1)}) fusion(bf16[1024,2048]{1,0:T(8,128)(2,1)} %param.20, bf16[2048,128]{1,0:T(8,128)(2,1)} %param.27), kind=kOutput, calls=%fused_computation.49 | convolution fusion | flops 537132032 | bytes 5246976 | tf_op jit(solution)/shard_map/dot_general | solution.py:140
  151.1 3.0 %all-to-all-done.1 = bf16[32,128,128]{2,1,0:T(8,128)(2,1)} async-done(((bf16[32,128,128]{2,1,0:T(8,128)(2,1)}), bf16[32,128,128]{2,1,0:T(8,128)(2,1)}, u32[]{:S(2)}, u32[]{:S(2)}) %all-to-all-start.1) | async-done | bytes 1048608 | tf_op jit(solution)/shard_map/all_to_all | solution.py:127
  154.1 2.0 %gather_fusion.1 = bf16[32,128,128]{2,1,0:T(8,128)(2,1)S(1)} fusion(bf16[32,128,128]{2,1,0:T(8,128)(2,1)} %all-to-all-done.1, s32[1024]{0:T(1024)S(1)} %pad_clamp_fusion), kind=kCustom, calls=%fused_computation.clone | custom fusion | bytes 2097280 | tf_op jit(solution)/shard_map/jit(_take)/gather | solution.py:132
  156.1 2.0 %select_convert_fusion = (f32[32,128,128]{2,1,0:T(8,128)}, bf16[32,128,128]{2,1,0:T(8,128)(2,1)}) fusion(bf16[32,128,128]{2,1,0:T(8,128)(2,1)S(1)} %gather_fusion.2, pred[32]{0:T(512)(128)(4,1)S(1)} %get-tuple-element.114, bf16[32,128,128]{2,1,0:T(8,128)(2,1)S(1)} %gather_fusion.1), kind=kLoop, calls=%fused_computation.43 | loop fusion | flops 1572864 | bytes 5242912 | tf_op jit(solution)/shard_map/convert_element_type | solution.py:137
  158.1 2.0 %fusion.8 = bf16[8,512,128]{2,1,0:T(8,128)(2,1)S(1)} fusion(f32[128]{0:T(128)S(1)} %copy-done.10, f32[8,512]{1,0:T(8,128)S(1)} %rsqrt.32, f32[8,512,128]{2,1,0:T(8,128)} %bitcast.141), kind=kLoop, calls=%fused_computation.19 | loop fusion | flops 1572864 | bytes 3162624 | tf_op jit(solution)/shard_map/convert_element_type | solution.py:138
  161.8 3.8 %multiply_reduce_fusion.1 = (f32[1024]{0:T(1024)S(1)}, f32[1024,128]{0,1:T(8,128)S(1)}) fusion(f32[1024,128]{0,1:T(8,128)S(1)} %copy.137, f32[1024,128]{0,1:T(8,128)S(1)} %copy.140, bf16[1024,2048]{1,0:T(8,128)(2,1)} %param.20, bf16[2048,128]{1,0:T(8,128)(2,1)S(1)} %copy-done.13), kind=kOutput, calls=%fused_computation.47 | convolution fusion | flops 537787392 | bytes 6295552 | tf_op jit(solution)/shard_map/dot_general | solution.py:153
  165.7 9.3 %all_to_all.22 = f32[8,1,1024]{2,1,0:T(1,128)S(1)} all-to-all(f32[8,1,1024]{2,1,0:T(1,128)S(1)} %broadcast_in_dim.88), channel_id=1, replica_groups=mesh['grp'=2,'st'=16,'tp'=8] {'tp'}, dimensions={0} | all-to-all | bytes 65536 | tf_op jit(solution)/shard_map/all_to_all | solution.py:19
  (109 shorter events, 26.9 us)
Async XLA Ops:
  0.0 81.2 %copy-start = (bf16[2048,128]{1,0:T(8,128)(2,1)S(1)}, bf16[2048,128]{1,0:T(8,128)(2,1)}, u32[]{:S(2)}) copy-start(bf16[2048,128]{1,0:T(8,128)(2,1)} %param.29) | copy-start | bytes 1572868
  3.0 58.7 %all-to-all-start = ((s32[16,1,2]{2,1,0:T(1,128)}), s32[16,1,2]{2,1,0:T(1,128)S(1)}, u32[]{:S(2)}, u32[]{:S(2)}) async-start(s32[16,1,2]{2,1,0:T(1,128)} %bitcast.12), calls=%async_computation | async-start | bytes 16384 | tf_op jit(solution)/shard_map/all_to_all | solution.py:114
  28.0 27.6 %copy-start.6 = (bf16[2048,128]{1,0:T(8,128)(2,1)S(1)}, bf16[2048,128]{1,0:T(8,128)(2,1)}, u32[]{:S(2)}) copy-start(bf16[2048,128]{1,0:T(8,128)(2,1)} %param.23) | copy-start | bytes 1572868
  32.0 27.2 %copy-start.7 = (bf16[2048,64]{0,1:T(8,128)(2,1)S(1)}, bf16[2048,64]{0,1:T(8,128)(2,1)}, u32[]{:S(2)}) copy-start(bf16[2048,64]{0,1:T(8,128)(2,1)} %param.21) | copy-start | bytes 786436
  55.6 3.6 %copy-start.2 = (bf16[1024,2048]{1,0:T(8,128)(2,1)S(1)}, bf16[1024,2048]{1,0:T(8,128)(2,1)}, u32[]{:S(2)}) copy-start(bf16[1024,2048]{1,0:T(8,128)(2,1)} %param.20) | copy-start | bytes 12582916
  81.2 6.1 %copy-start.3 = (bf16[4096,2048]{1,0:T(8,128)(2,1)}, bf16[4096,2048]{1,0:T(8,128)(2,1)S(1)}, u32[]{:S(2)}) copy-start(bf16[4096,2048]{1,0:T(8,128)(2,1)S(1)} %bitcast_select_fusion) | copy-start | bytes 50331652
  81.2 13.4 %copy-start.8 = (bf16[2048,64]{0,1:T(8,128)(2,1)S(1)}, bf16[2048,64]{0,1:T(8,128)(2,1)}, u32[]{:S(2)}) copy-start(bf16[2048,64]{0,1:T(8,128)(2,1)} %param.22) | copy-start | bytes 786436
  87.3 35.3 %all-to-all-start.2 = ((bf16[32,128,128]{2,1,0:T(8,128)(2,1)}), bf16[32,128,128]{2,1,0:T(8,128)(2,1)S(1)}, u32[]{:S(2)}, u32[]{:S(2)}) async-start(bf16[32,128,128]{2,1,0:T(8,128)(2,1)} %bitcast.150), calls=%async_computation.2 | async-start | bytes 2097152 | tf_op jit(solution)/shard_map/all_to_all | solution.py:126
  94.6 4.4 %copy-start.4 = (f32[8,128,1,64]{3,0,1,2:T(8,128)S(1)}, f32[8,128,1,64]{3,0,1,2:T(8,128)}, u32[]{:S(2)}) copy-start(f32[8,128,1,64]{3,0,1,2:T(8,128)} %copy.127) | copy-start | bytes 786436
  94.7 5.2 %copy-start.12 = (bf16[2048,128]{1,0:T(8,128)(2,1)S(1)}, bf16[2048,128]{1,0:T(8,128)(2,1)}, u32[]{:S(2)}) copy-start(bf16[2048,128]{1,0:T(8,128)(2,1)} %param.30) | copy-start | bytes 1572868
  122.6 31.5 %all-to-all-start.1 = ((bf16[32,128,128]{2,1,0:T(8,128)(2,1)}), bf16[32,128,128]{2,1,0:T(8,128)(2,1)}, u32[]{:S(2)}, u32[]{:S(2)}) async-start(bf16[32,128,128]{2,1,0:T(8,128)(2,1)} %bitcast.149), calls=%async_computation.1 | async-start | bytes 2097152 | tf_op jit(solution)/shard_map/all_to_all | solution.py:127
  150.4 7.7 %copy-start.10 = (f32[128]{0:T(128)S(1)}, f32[128]{0:T(128)}, u32[]{:S(2)}) copy-start(f32[128]{0:T(128)} %param.32) | copy-start | bytes 1540
  156.1 4.1 %copy-start.11 = (f32[128]{0:T(128)S(1)}, f32[128]{0:T(128)}, u32[]{:S(2)}) copy-start(f32[128]{0:T(128)} %param.31) | copy-start | bytes 1540
  158.1 2.7 %copy-start.5 = (bf16[32,128,128]{2,1,0:T(8,128)(2,1)S(1)}, bf16[32,128,128]{2,1,0:T(8,128)(2,1)}, u32[]{:S(2)}) copy-start(bf16[32,128,128]{2,1,0:T(8,128)(2,1)} %get-tuple-element.121) | copy-start | bytes 3145732
  160.8 1.0 copy-start.13
  161.4 14.6 %copy-start.1 = (bf16[2048,128]{1,0:T(8,128)(2,1)S(1)}, bf16[2048,128]{1,0:T(8,128)(2,1)}, u32[]{:S(2)}) copy-start(bf16[2048,128]{1,0:T(8,128)(2,1)} %param.29) | copy-start | bytes 1572868
  161.8 13.2 %copy-start.9 = (f32[128]{0:T(128)S(1)}, f32[128]{0:T(128)}, u32[]{:S(2)}) copy-start(f32[128]{0:T(128)} %param.33) | copy-start | bytes 1540
where the time goes:
time: 177 us; the launch traced here: 176 us
  matrix products  46.1 us (26%)
  other arithmetic  41.3 us (23%)
  starting transfers between devices  35.5 us (20%)
  local copies, waits for them, and re-layouts  26.8 us (15%)
  waiting for transfers between devices  16.5 us (9%)
  blocking collectives  9.31 us (5%)
    all_to_all x1, starting transfers between devices, on_device(): lax.all_to_all(wanted.reshape(st_size, most), 'st', split_axis=0, concat_...  23.7 us
    another operation x1, other arithmetic, gla_blocks(): cumulative = jnp.cumsum(log_decay, axis=1)  23.3 us
    all_to_all x1, waiting for transfers between devices, on_device(): lax.all_to_all(made_keys, 'st', split_axis=0, concat_axis=0, tiled=True)  13.6 us
    gather x1, local copies, waits for them, and re-layouts, on_device(): held_rows = jnp.take(store, jnp.maximum(incoming.reshape(-1), 0), axis=0)  10 us
    all_to_all x1, blocking collectives, sent_to_all(): return lax.all_to_all(copies, axis, split_axis=0, concat_axis=0, tiled=True)  9.31 us
    dot_general x1, matrix products, on_device(): jnp.dot(flat_rows, w_rvalue, preferred_element_type=jnp.float32)  9.2 us
    select_n x1, other arithmetic, on_device(): held_rows = jnp.take(store, jnp.maximum(incoming.reshape(-1), 0), axis=0)  9.14 us
    dynamic_slice x8, local copies, waits for them, and re-layouts, gla_blocks(): lax.scan(advance, start_state, (query_dec, update, carry_decay))  8.73 us
  transfers between devices with their start and end apart: 3, of which 2 were waited for; matrix products, arithmetic and copies ran while one was open for 42% of the time, Pallas kernels for 0%

commit v1 on v0

v1 whole, which is shorter than its diff:
```python
import functools

import jax
import jax.numpy as jnp
from jax import lax
from jax.experimental import pallas as pl
from jax.experimental.pallas import tpu as pltpu
from jax.sharding import PartitionSpec as P

HEADS = 8
DK = 64
DV = 128
BLK = 128
NPASS = 4
EPS = 1e-06
PRECISE = lax.Precision.HIGHEST
F32 = jnp.float32
BF16 = jnp.bfloat16


def nt(a, b, precision=None):
    return lax.dot_general(a, b, (((1,), (1,)), ((), ())), precision=precision, preferred_element_type=F32)


def head_norm(values, gain_row):
    return values * lax.rsqrt(jnp.mean(values * values, axis=-1, keepdims=True) + EPS) * gain_row


def requests_kernel(here, most, ids_ref, wanted_ref, slot_ref, count_ref):
    owners = count_ref.shape[0]

    def clear(i, _):
        count_ref[i] = 0
        return 0

    lax.fori_loop(0, owners, clear, 0)
    blocks, passes = ids_ref.shape

    def one(i, _):
        wanted = ids_ref[i // passes, i % passes]
        owner = jnp.clip(lax.div(wanted, jnp.int32(here)), 0, owners - 1)
        rank = jnp.minimum(count_ref[owner], most - 1)
        count_ref[owner] = rank + 1
        wanted_ref[owner, rank] = wanted - owner * here
        slot_ref[i] = owner * most + rank
        return 0

    lax.fori_loop(0, blocks * passes, one, 0)


def passages_kernel(store_ref, wk_ref, wv_ref, gain_ref, out_ref, weight_ref):
    @pl.when(pl.program_id(0) == 0)
    def _():
        weight_ref[:, :DV] = wk_ref[...]
        weight_ref[:, DV:] = wv_ref[...]

    count, rows, width = store_ref.shape
    made = jnp.dot(store_ref[...].reshape(count * rows, width), weight_ref[...], preferred_element_type=F32)
    made = made.astype(BF16)
    keys = head_norm(made[:, :DV].astype(F32), gain_ref[...]).astype(BF16)
    out_ref[:, :, :DV] = keys.reshape(count, rows, DV)
    out_ref[:, :, DV:] = made[:, DV:].reshape(count, rows, DV)


def pack_kernel(wanted_ref, made_ref, out_ref, sems):
    held = made_ref.shape[0]
    most = wanted_ref.shape[1]

    def copy(i):
        row = jnp.clip(wanted_ref[i // most, i % most], 0, held - 1)
        return pltpu.make_async_copy(made_ref.at[row], out_ref.at[i], sems.at[i])

    count = out_ref.shape[0]
    for i in range(count):
        copy(i).start()
    for i in range(count):
        copy(i).wait()


def tokens_kernel(
    after_ref,
    scale_ref,
    tok_ref,
    wq_ref,
    wk_ref,
    wv_ref,
    wd_ref,
    wr_ref,
    wg_ref,
    rate_ref,
    qgain_ref,
    gla_ref,
    gate_ref,
    rq_ref,
    state_ref,
):
    step = pl.program_id(0)

    @pl.when(step == 0)
    def _():
        state_ref[...] = jnp.zeros_like(state_ref)

    tokens = tok_ref[...]
    rows = tokens.shape[0]

    def times(w_ref):
        return jnp.dot(tokens, w_ref[...], preferred_element_type=F32)

    query = times(wq_ref)
    key = times(wk_ref)
    value = times(wv_ref)
    decay = times(wd_ref)
    rq_ref[...] = head_norm(times(wr_ref), qgain_ref[...]).astype(BF16)
    gate_ref[...] = jax.nn.sigmoid(times(wg_ref))
    row_id = lax.broadcasted_iota(jnp.int32, (BLK, BLK), 0)
    col_id = lax.broadcasted_iota(jnp.int32, (BLK, BLK), 1)
    causal = row_id >= col_id
    lower = causal.astype(F32)
    for b in range(rows // BLK):
        at = slice(b * BLK, (b + 1) * BLK)
        log_decay = -2.0 * rate_ref[...] * jax.nn.sigmoid(decay[at]) * scale_ref[step * (rows // BLK) + b]
        total = jnp.dot(lower, log_decay, precision=PRECISE, preferred_element_type=F32)
        last = total[BLK - 1 : BLK]
        q_dec = query[at] * DK ** (-0.5) * jnp.exp(total)
        k_dec = key[at] * jnp.exp(-total)
        scores = jnp.where(causal, nt(q_dec, k_dec, PRECISE), 0.0)
        within = jnp.dot(scores, value[at], precision=PRECISE, preferred_element_type=F32)
        gla_ref[at] = within + nt(q_dec, state_ref[...], PRECISE)
        update = lax.dot_general(
            value[at],
            key[at] * jnp.exp(last - total),
            (((0,), (0,)), ((), ())),
            precision=PRECISE,
            preferred_element_type=F32,
        )
        state_ref[...] = state_ref[...] * jnp.exp(last) + update


def reads_kernel(slot_ref, got_ref, rq_ref, gla_ref, gate_ref, out_ref, square_ref, held_ref, sems):
    step = pl.program_id(0)
    count = got_ref.shape[0]

    def copy(i):
        slot = jnp.clip(slot_ref[i], 0, count - 1)
        return pltpu.make_async_copy(got_ref.at[slot], held_ref.at[i], sems.at[i])

    @pl.when(step == 0)
    def _():
        for i in range(count):
            copy(i).start()

    for j in range(NPASS):
        copy(step * NPASS + j).wait()
    query = rq_ref[...]
    first = step * NPASS
    rows = held_ref.shape[1]
    parts = []
    for j in range(NPASS):
        parts.append(jnp.exp(nt(query, held_ref[first + j, :, :DV]) * DV ** (-0.5)))
    bottom = sum(jnp.sum(p, axis=-1, keepdims=True) for p in parts)
    read = jnp.zeros((query.shape[0], DV), F32)
    for j in range(NPASS):
        weight = (parts[j] / bottom).astype(BF16)
        read += jnp.dot(weight, held_ref[first + j, :, DV:], preferred_element_type=F32)
    combined = gla_ref[...] + gate_ref[...] * read
    out_ref[...] = combined
    sums = nt(jnp.ones((8, DV), F32), combined * combined, PRECISE)
    square_ref[...] = jnp.broadcast_to(sums[0:1].reshape(1, 1, 1, BLK), square_ref.shape)


def scale_kernel(square_ref, combined_ref, gain_ref, out_ref):
    total = jnp.sum(square_ref[...], axis=0)[:, 0, :]
    scale = lax.rsqrt(total / (HEADS * DV) + EPS)
    columns = jnp.transpose(scale)
    for b in range(total.shape[0]):
        at = slice(b * BLK, (b + 1) * BLK)
        out_ref[at] = (combined_ref[at] * columns[:, b : b + 1] * gain_ref[...]).astype(BF16)


VMEM = pl.BlockSpec(memory_space=pltpu.VMEM)
SMEM = pl.BlockSpec(memory_space=pltpu.SMEM)
ANY = pl.BlockSpec(memory_space=pl.ANY)


def whole(shape):
    return pl.BlockSpec(shape, lambda i: (0,) * len(shape))


def on_device(
    tokens,
    w_query,
    w_key,
    w_value,
    w_decay,
    decay_rate,
    block_scale,
    w_rquery,
    w_gate,
    w_rkey,
    w_rvalue,
    query_gain,
    key_gain,
    out_gain,
    store,
    passage_ids,
):
    length, width = tokens.shape
    blocks = length // BLK
    held, plen, _ = store.shape
    st_size = lax.axis_size("st")
    tp_size = lax.axis_size("tp")
    requests = passage_ids.shape[0] * passage_ids.shape[1]
    owners = min(st_size, requests // 2)
    most = requests // owners
    slots = st_size * most

    wanted, slot_index = pl.pallas_call(
        functools.partial(requests_kernel, held, most),
        out_shape=(
            jax.ShapeDtypeStruct((st_size, most), jnp.int32),
            jax.ShapeDtypeStruct((requests,), jnp.int32),
        ),
        in_specs=[SMEM],
        out_specs=(SMEM, SMEM),
        scratch_shapes=[pltpu.SMEM((st_size,), jnp.int32)],
        name="requests",
    )(passage_ids)
    incoming = lax.all_to_all(wanted, "st", split_axis=0, concat_axis=0, tiled=True)

    step_passages = 2
    made = pl.pallas_call(
        passages_kernel,
        grid=(held // step_passages,),
        out_shape=jax.ShapeDtypeStruct((held, plen, 2 * DV), BF16),
        in_specs=[
            pl.BlockSpec((step_passages, plen, width), lambda i: (i, 0, 0)),
            whole((width, DV)),
            whole((width, DV)),
            whole((1, DV)),
        ],
        out_specs=pl.BlockSpec((step_passages, plen, 2 * DV), lambda i: (i, 0, 0)),
        scratch_shapes=[pltpu.VMEM((width, 2 * DV), BF16)],
        cost_estimate=pl.CostEstimate(
            flops=2 * held * plen * width * 2 * DV,
            bytes_accessed=2 * held * plen * (width + 2 * DV),
            transcendentals=0,
        ),
        name="passages",
    )(store, w_rkey, w_rvalue, key_gain.reshape(1, DV))

    packed = pl.pallas_call(
        pack_kernel,
        out_shape=jax.ShapeDtypeStruct((slots, plen, 2 * DV), BF16),
        in_specs=[SMEM, VMEM],
        out_specs=ANY,
        scratch_shapes=[pltpu.SemaphoreType.DMA((slots,))],
        name="pack",
    )(incoming, made)
    got = lax.all_to_all(packed, "st", split_axis=0, concat_axis=0, tiled=True)

    rows = 2 * BLK
    gla, gate, read_query = pl.pallas_call(
        tokens_kernel,
        grid=(length // rows,),
        out_shape=(
            jax.ShapeDtypeStruct((length, DV), F32),
            jax.ShapeDtypeStruct((length, DV), F32),
            jax.ShapeDtypeStruct((length, DV), BF16),
        ),
        in_specs=[
            ANY,
            SMEM,
            pl.BlockSpec((rows, width), lambda i: (i, 0)),
            whole((width, DK)),
            whole((width, DK)),
            whole((width, DV)),
            whole((width, DK)),
            whole((width, DV)),
            whole((width, DV)),
            whole((1, DK)),
            whole((1, DV)),
        ],
        out_specs=(
            pl.BlockSpec((rows, DV), lambda i: (i, 0)),
            pl.BlockSpec((rows, DV), lambda i: (i, 0)),
            pl.BlockSpec((rows, DV), lambda i: (i, 0)),
        ),
        scratch_shapes=[pltpu.VMEM((DV, DK), F32)],
        cost_estimate=pl.CostEstimate(
            flops=20 * length * width * (3 * DK + 3 * DV), bytes_accessed=2 * length * width, transcendentals=0
        ),
        name="tokens",
    )(
        packed,
        block_scale,
        tokens,
        w_query,
        w_key,
        w_value,
        w_decay,
        w_rquery,
        w_gate,
        decay_rate.reshape(1, DK),
        query_gain.reshape(1, DV),
    )

    combined, squares = pl.pallas_call(
        reads_kernel,
        grid=(blocks,),
        out_shape=(
            jax.ShapeDtypeStruct((length, DV), F32),
            jax.ShapeDtypeStruct((tp_size, blocks, 1, BLK), F32),
        ),
        in_specs=[
            SMEM,
            ANY,
            pl.BlockSpec((BLK, DV), lambda i: (i, 0)),
            pl.BlockSpec((BLK, DV), lambda i: (i, 0)),
            pl.BlockSpec((BLK, DV), lambda i: (i, 0)),
        ],
        out_specs=(
            pl.BlockSpec((BLK, DV), lambda i: (i, 0)),
            pl.BlockSpec((tp_size, 1, 1, BLK), lambda i: (0, i, 0, 0)),
        ),
        scratch_shapes=[pltpu.VMEM((slots, plen, 2 * DV), BF16), pltpu.SemaphoreType.DMA((slots,))],
        name="reads",
    )(slot_index, got, read_query, gla, gate)
    everyone = lax.all_to_all(squares, "tp", split_axis=0, concat_axis=0, tiled=True)

    return pl.pallas_call(
        scale_kernel,
        out_shape=jax.ShapeDtypeStruct((length, DV), BF16),
        in_specs=[VMEM, VMEM, VMEM],
        out_specs=VMEM,
        name="scale",
    )(everyone, combined, out_gain.reshape(1, DV))


def solution(mesh):
    return jax.shard_map(
        on_device,
        mesh=mesh,
        in_specs=(
            P(("grp", "st"), None),
            P(None, "tp"),
            P(None, "tp"),
            P(None, "tp"),
            P(None, "tp"),
            P("tp"),
            P(("grp", "st")),
            P(None, "tp"),
            P(None, "tp"),
            P(None, "tp"),
            P(None, "tp"),
            P(),
            P(),
            P("tp"),
            P(("grp", "st"), None, None),
            P(("grp", "st"), None),
        ),
        out_specs=P(("grp", "st"), "tp"),
        check_vma=False,
    )
```

time: 177 us -> 119 us (0.67)
  matrix products: 46.1 us -> 0 us
  other arithmetic: 41.3 us -> 0 us
  Pallas kernels: 0 us -> 39.1 us
  local copies, waits for them, and re-layouts: 26.8 us -> 6.32 us
  waiting for transfers between devices: 16.5 us -> 30.8 us
  starting transfers between devices: 35.5 us -> 31.1 us
    dot_general x21 -> x0, matrix products: 46.1 us -> none  [the longest x1 9.2 us: on_device(): jnp.dot(flat_rows, w_rvalue, preferred_element_type=jnp.float32)]
    pallas_call x0 -> x6, Pallas kernels: none -> 39.1 us  [the longest x1 15.2 us: on_device(): pl.pallas_call(tokens_kernel, grid=(length // rows,), out_shape=(jax.Shap...]
    another operation x1 -> x0, other arithmetic: 23.3 us -> none  [gla_blocks(): cumulative = jnp.cumsum(log_decay, axis=1)]
    all_to_all x3 -> x2, waiting for transfers between devices: 16.5 us -> 30.8 us  [the longest x1 30.8 us: on_device(): got = lax.all_to_all(packed, 'st', split_axis=0, concat_axis=0, tiled=True)]
    gather x3 -> x0, local copies, waits for them, and re-layouts: 12.7 us -> none  [the longest x1 10 us: on_device(): held_rows = jnp.take(store, jnp.maximum(incoming.reshape(-1), 0), axis=0)]
    select_n x3 -> x0, other arithmetic: 9.15 us -> none  [the longest x1 9.14 us: on_device(): held_rows = jnp.take(store, jnp.maximum(incoming.reshape(-1), 0), axis=0)]
    dynamic_slice x8 -> x0, local copies, waits for them, and re-layouts: 8.73 us -> none  [gla_blocks(): lax.scan(advance, start_state, (query_dec, update, carry_decay))]
    unnamed x30 -> x14, local copies, waits for them, and re-layouts: 0.4 us -> 6.32 us
  transfers between devices with their start and end apart: 3 -> 2, of which waited for: 2 -> 1; matrix products, arithmetic and copies ran while one was open for 42% -> 3% of each run, Pallas kernels for 0% -> 19%
where the time goes in v1:
time: 119 us; the launch traced here: 118 us
  Pallas kernels  39.1 us (33%)
  starting transfers between devices  31.1 us (26%)
  waiting for transfers between devices  30.8 us (26%)
  blocking collectives  10.9 us (9%)
  local copies, waits for them, and re-layouts  6.32 us (5%)
    all_to_all x1, waiting for transfers between devices, on_device(): got = lax.all_to_all(packed, 'st', split_axis=0, concat_axis=0, tiled=True)  30.8 us
    all_to_all x1, starting transfers between devices, on_device(): lax.all_to_all(wanted, 'st', split_axis=0, concat_axis=0, tiled=True)  23.7 us
    pallas_call x1, Pallas kernels, on_device(): pl.pallas_call(tokens_kernel, grid=(length // rows,), out_shape=(jax.Shap...  15.2 us
    all_to_all x1, blocking collectives, on_device(): lax.all_to_all(squares, 'tp', split_axis=0, concat_axis=0, tiled=True)  10.9 us
    pallas_call x1, Pallas kernels, on_device(): pl.pallas_call(reads_kernel, grid=(blocks,), out_shape=(jax.ShapeDtypeStr...  9.45 us
    all_to_all x1, starting transfers between devices, on_device(): got = lax.all_to_all(packed, 'st', split_axis=0, concat_axis=0, tiled=True)  7.39 us
    pallas_call x1, Pallas kernels, on_device(): pl.pallas_call(passages_kernel, grid=(held // step_passages,), out_shape=...  7.28 us
    unnamed x14, local copies, waits for them, and re-layouts  6.32 us
  transfers between devices with their start and end apart: 2, of which 1 were waited for; matrix products, arithmetic and copies ran while one was open for 3% of the time, Pallas kernels for 19%

profile of v1, /device:TPU:513, one launch (start us, length us, event | category | flops | bytes accessed | tf_op | source)
XLA Modules:
  0.0 118.2 jit_solution(4856464816755572502)
XLA Ops:
  0.0 1.3 %copy.23.ids_ref = s32[8,4]{1,0:T(8,128)} copy(s32[8,4]{0,1:T(4,128)} %param.31) | data formatting | bytes 256 | tf_op args[15]
  1.3 2.3 %requests.1 = (s32[16,2]{1,0:T(8,128)}, s32[32]{0:T(128)}) custom-call(s32[8,4]{1,0:T(8,128)} %copy.23.ids_ref), custom_call_target="tpu_custom_call" | custom-call | tf_op jit(solution)/shard_map/requests/pallas_call | solution.py:217
  3.6 23.7 %all-to-all-start = ((s32[16,1,2]{2,1,0:T(1,128)}), s32[16,1,2]{2,1,0:T(1,128)S(1)}, u32[]{:S(2)}, u32[]{:S(2)}) async-start(s32[16,1,2]{2,1,0:T(1,128)} %bitcast.9), calls=%async_computation | async-start | bytes 16384 | tf_op jit(solution)/shard_map/all_to_all | solution.py:228
  27.3 7.3 %passages.1.made_ref = bf16[12,128,256]{2,1,0:T(8,128)(2,1)} custom-call(bf16[12,128,2048]{2,1,0:T(8,128)(2,1)} %store_ref.1, bf16[2048,128]{1,0:T(8,128)(2,1)} %wk_ref.2, bf16[2048,128]{1,0:T(8,128)(2,1)} %wv_ref.2, f32[1,128]{1,0:T(1,128)} %bitcast.10), custom_call_target="tpu_custom_call" | custom-call | flops 1610612736 | bytes 7077888 | tf_op jit(solution)/shard_map/passages/pallas_call | solution.py:231
  34.6 0.0 copy-start.2
  34.6 0.0 all-to-all-done
  34.6 0.0 copy-start.4
  34.6 0.6 copy-done.4
  35.2 0.0 copy-start.3
  35.2 2.8 %pack.1.after_ref = bf16[32,128,256]{2,1,0:T(8,128)(2,1)} custom-call(s32[16,2]{1,0:T(8,128)} %bitcast.8, bf16[12,128,256]{2,1,0:T(8,128)(2,1)} %passages.1.made_ref), custom_call_target="tpu_custom_call" | custom-call | tf_op jit(solution)/shard_map/pack/pallas_call | solution.py:251
  38.0 7.4 %all-to-all-start.1 = ((bf16[32,128,256]{2,1,0:T(8,128)(2,1)}), bf16[32,128,256]{2,1,0:T(8,128)(2,1)S(1)}, u32[]{:S(2)}, u32[]{:S(2)}) async-start(bf16[32,128,256]{2,1,0:T(8,128)(2,1)} %pack.1.after_ref), calls=%async_computation.1 | async-start | bytes 4194304 | tf_op jit(solution)/shard_map/all_to_all | solution.py:259
  45.4 0.0 copy-done.1
  45.4 1.0 copy.28.wq_ref
  46.5 0.0 copy-done.2
  46.5 1.0 copy.29.wk_ref
  47.5 0.0 copy-done.3
  47.5 1.0 copy.30.wd_ref
  48.5 15.2 %tokens.1 = (f32[1024,128]{1,0:T(8,128)}, f32[1024,128]{1,0:T(8,128)}, bf16[1024,128]{1,0:T(8,128)(2,1)}) custom-call(bf16[32,128,256]{2,1,0:T(8,128)(2,1)} %pack.1.after_ref, f32[8]{0:T(128)} %scale_ref.1, bf16[1024,2048]{1,0:T(8,128)(2,1)} %tok_ref.1, bf16[2048,64]{1,0:T(8,128)(2,1)} %copy.28.wq_ref, bf16[2048,64]{1,0:T(8,128)(2,1)} %copy.29.wk_ref, ...), custom_call_target="tpu_custom_call" | custom-call | flops 24159191040 | bytes 4194304 | tf_op jit(solution)/shard_map/tokens/pallas_call | solution.py:262
  63.7 30.8 %all-to-all-done.1.got_ref = bf16[32,128,256]{2,1,0:T(8,128)(2,1)S(1)} async-done(((bf16[32,128,256]{2,1,0:T(8,128)(2,1)}), bf16[32,128,256]{2,1,0:T(8,128)(2,1)S(1)}, u32[]{:S(2)}, u32[]{:S(2)}) %all-to-all-start.1) | async-done | bytes 2097184 | tf_op jit(solution)/shard_map/all_to_all | solution.py:259
  94.5 0.0 copy-start
  94.5 1.3 %copy-done = bf16[32,128,256]{2,1,0:T(8,128)(2,1)} copy-done((bf16[32,128,256]{2,1,0:T(8,128)(2,1)}, bf16[32,128,256]{2,1,0:T(8,128)(2,1)S(1)}, u32[]{:S(2)}) %copy-start) | copy-done | bytes 2097176
  95.8 9.4 %reads.1 = (f32[1024,128]{1,0:T(8,128)}, f32[8,8,1,128]{3,2,1,0:T(1,128)}) custom-call(s32[32]{0:T(128)} %get-tuple-element.12.slot_ref, bf16[32,128,256]{2,1,0:T(8,128)(2,1)} %copy-done, bf16[1024,128]{1,0:T(8,128)(2,1)} %get-tuple-element.14.rq_ref, f32[1024,128]{1,0:T(8,128)} %get-tuple-element.15.gla_ref, f32[1024,128]{1,0:T(8,128)} %get-tuple-element.16.gate_ref), custom_call_target="tpu_custom_call" | custom-call | tf_op jit(solution)/shard_map/reads/pallas_call | solution.py:307
  105.2 10.9 %all_to_all.21.square_ref = f32[8,8,1,128]{3,2,1,0:T(1,128)} all-to-all(f32[8,8,1,128]{3,2,1,0:T(1,128)} %get-tuple-element.17), channel_id=1, replica_groups=mesh['grp'=2,'st'=16,'tp'=8] {'tp'}, dimensions={0} | all-to-all | bytes 65536 | tf_op jit(solution)/shard_map/all_to_all | solution.py:328
  116.1 2.1 %scale.1 = bf16[1024,128]{1,0:T(8,128)(2,1)} custom-call(f32[8,8,1,128]{3,2,1,0:T(1,128)} %all_to_all.21.square_ref, f32[1024,128]{1,0:T(8,128)} %get-tuple-element.18.combined_ref, f32[1,128]{1,0:T(1,128)} %bitcast.11), custom_call_target="tpu_custom_call" | custom-call | tf_op jit(solution)/shard_map/scale/pallas_call | solution.py:330
  (1 shorter events, 0.0 us)
Async XLA Ops:
  3.6 31.0 %all-to-all-start = ((s32[16,1,2]{2,1,0:T(1,128)}), s32[16,1,2]{2,1,0:T(1,128)S(1)}, u32[]{:S(2)}, u32[]{:S(2)}) async-start(s32[16,1,2]{2,1,0:T(1,128)} %bitcast.9), calls=%async_computation | async-start | bytes 16384 | tf_op jit(solution)/shard_map/all_to_all | solution.py:228
  34.6 10.8 %copy-start.1 = (bf16[2048,64]{0,1:T(8,128)(2,1)S(1)}, bf16[2048,64]{0,1:T(8,128)(2,1)}, u32[]{:S(2)}) copy-start(bf16[2048,64]{0,1:T(8,128)(2,1)} %param.17) | copy-start | bytes 786436
  34.6 11.9 %copy-start.2 = (bf16[2048,64]{0,1:T(8,128)(2,1)S(1)}, bf16[2048,64]{0,1:T(8,128)(2,1)}, u32[]{:S(2)}) copy-start(bf16[2048,64]{0,1:T(8,128)(2,1)} %param.18) | copy-start | bytes 786436
  34.6 0.6 copy-start.4
  35.2 12.3 %copy-start.3 = (bf16[2048,64]{0,1:T(8,128)(2,1)S(1)}, bf16[2048,64]{0,1:T(8,128)(2,1)}, u32[]{:S(2)}) copy-start(bf16[2048,64]{0,1:T(8,128)(2,1)} %param.20) | copy-start | bytes 786436
  38.0 56.4 %all-to-all-start.1 = ((bf16[32,128,256]{2,1,0:T(8,128)(2,1)}), bf16[32,128,256]{2,1,0:T(8,128)(2,1)S(1)}, u32[]{:S(2)}, u32[]{:S(2)}) async-start(bf16[32,128,256]{2,1,0:T(8,128)(2,1)} %pack.1.after_ref), calls=%async_computation.1 | async-start | bytes 4194304 | tf_op jit(solution)/shard_map/all_to_all | solution.py:259
  94.5 1.3 %copy-start = (bf16[32,128,256]{2,1,0:T(8,128)(2,1)}, bf16[32,128,256]{2,1,0:T(8,128)(2,1)S(1)}, u32[]{:S(2)}) copy-start(bf16[32,128,256]{2,1,0:T(8,128)(2,1)S(1)} %all-to-all-done.1.got_ref) | copy-start | bytes 6291460
